TPU v7x, 32 devices: a whole 2x2x4 slice. The times are simulated.
32 devices in a mesh: sp: 4 (over z), fs: 4 (over y, x), tp: 2 (over core).
Axes of the slice: x: 2, y: 2, z: 4, core: 2. Of those that a mesh axis runs over, the one named last changes fastest.
Arguments:
- tokens: bfloat16 [4, 512, 4096], P('fs', 'sp', 'tp'), may hold values from -6 to 6
- norm_gain: float32 [4096], replicated, may hold values from 0.1 to 1.9
- w_state_in: bfloat16 [4096, 2048], P(('sp', 'fs'), 'tp'), may hold values from -0.09375 to 0.09375
- w_query: bfloat16 [4096, 2048], P(('sp', 'fs'), 'tp'), may hold values from -0.3125 to 0.3125
- w_key: bfloat16 [4096, 2048], P(('sp', 'fs'), 'tp'), may hold values from -0.3125 to 0.3125
- w_value: bfloat16 [4096, 2048], P(('sp', 'fs'), 'tp'), may hold values from -0.09375 to 0.09375
- decay_re: float32 [128, 64], P('tp'), may hold values from -0.034 to -9.765625e-05
- decay_im: float32 [128, 64], P('tp'), may hold values from -3.140625 to 3.140625
- log_step: float32 [128], P('tp'), may hold values from -3.5 to -1.5
- decay_shift: float32 [4, 128, 512], P('fs', 'tp', 'sp'), may hold values from -2 to 0
- in_re: float32 [128, 64, 16], P('tp'), may hold values from -2 to 2
- in_im: float32 [128, 64, 16], P('tp'), may hold values from -2 to 2
- output_real: float32 [128, 16, 64], P('tp'), may hold values from -0.75 to 0.75
- output_imaginary: float32 [128, 16, 64], P('tp'), may hold values from -0.75 to 0.75
- skip: float32 [2048], P('tp'), may hold values from -1.2 to 1.2
- mix_weight: float32 [8], P('tp'), may hold values from 0.3 to 0.8
- head_gain: float32 [256], replicated, may hold values from 0.1 to 1.9
- w_out_state: bfloat16 [2048, 4096], P('tp'), may hold values from -0.125 to 0.125
- w_out_attn: bfloat16 [2048, 4096], P('tp'), may hold values from -0.125 to 0.125
Outputs:
- mixed: bfloat16 [4, 512, 4096], P('fs', ('sp', 'tp'))
- log_totals: float32 [4, 8, 2, 512], P('fs', 'tp', None, 'sp')
All inputs are finite; a program needn't handle non-finite values.
Results may differ from a plain program's by a relative error of at most 0.015.
Values may be sent and summed in bfloat16 or wider, within the bound.
A program may use at most 128 MiB of HBM per device.

v0:
```python
import math

import jax
import jax.numpy as jnp
from jax import lax
from jax.sharding import PartitionSpec as P


def prefix(x, axis, combine, identity):
    size, here = (lax.axis_size(axis), lax.axis_index(axis))
    everything = jax.tree.map(lambda part: lax.all_gather(part, axis), x)
    start = jax.tree.map(
        lambda part, zero: jnp.broadcast_to(jnp.asarray(zero, part.dtype), part.shape), x, identity
    )

    def hop(k, before):
        reached = k < here
        new = combine(before, jax.tree.map(lambda part: part[k], everything))
        return jax.tree.map(lambda a, b: jnp.where(reached, a, b), new, before)

    return lax.fori_loop(0, size, hop, start)


def compose(earlier, later):
    early_scale_re, early_scale_im, early_shift_re, early_shift_im = earlier
    late_scale_re, late_scale_im, late_shift_re, late_shift_im = later
    scale_re = late_scale_re * early_scale_re - late_scale_im * early_scale_im
    scale_im = late_scale_re * early_scale_im + late_scale_im * early_scale_re
    shift_re = late_scale_re * early_shift_re - late_scale_im * early_shift_im + late_shift_re
    shift_im = late_scale_re * early_shift_im + late_scale_im * early_shift_re + late_shift_im
    return (scale_re, scale_im, shift_re, shift_im)


def state_branch(
    state_in,
    decay_re,
    decay_im,
    log_step,
    decay_shift,
    in_re,
    in_im,
    output_real,
    output_imaginary,
    skip,
):
    upper_limit = lax.Precision.HIGHEST
    tok_rows = state_in.shape[0]
    group_count, state_size = decay_re.shape
    group_width = in_re.shape[2]
    flat_width = group_count * state_size
    step_size = jnp.exp(log_step)[:, None]
    numer_re = jnp.expm1(decay_re) * jnp.cos(decay_im) - 2.0 * jnp.sin(0.5 * decay_im) ** 2
    numer_im = jnp.exp(decay_re) * jnp.sin(decay_im)
    modulus = decay_re * decay_re + decay_im * decay_im
    coef_re = step_size * (numer_re * decay_re + numer_im * decay_im) / modulus
    coef_im = step_size * (numer_im * decay_re - numer_re * decay_im) / modulus
    matrix_re = coef_re[..., None] * in_re - coef_im[..., None] * in_im
    matrix_im = coef_re[..., None] * in_im + coef_im[..., None] * in_re
    inputs = state_in.astype(jnp.float32).reshape(tok_rows, group_count, group_width)
    flat_shape = (tok_rows, flat_width)
    drive_re = jnp.einsum("gpc,tgc->tgp", matrix_re, inputs, precision=upper_limit).reshape(
        flat_shape
    )
    drive_im = jnp.einsum("gpc,tgc->tgp", matrix_im, inputs, precision=upper_limit).reshape(
        flat_shape
    )
    magnitude = jnp.exp(decay_re[None] + decay_shift[0].T[:, :, None])
    factor_re = (magnitude * jnp.cos(decay_im)[None]).reshape(flat_shape)
    factor_im = (magnitude * jnp.sin(decay_im)[None]).reshape(flat_shape)
    span = math.gcd(tok_rows, 16)
    block_count = tok_rows // span

    def to_blocks(values):
        return values.reshape(block_count, span, flat_width).transpose(1, 0, 2)

    rows_in = tuple((to_blocks(values) for values in (factor_re, factor_im, drive_re, drive_im)))
    ones_blocks = jnp.ones((block_count, flat_width), jnp.float32)
    zero_blocks = jnp.zeros((block_count, flat_width), jnp.float32)

    def row_step(carry, row):
        joined = compose(carry, row)
        return (joined, joined)

    block_totals, local = lax.scan(
        row_step, (ones_blocks, zero_blocks, zero_blocks, zero_blocks), rows_in
    )
    ones_row = jnp.ones((flat_width,), jnp.float32)
    zero_row = jnp.zeros((flat_width,), jnp.float32)

    def block_step(carry, row):
        return (compose(carry, row), carry)

    totals, before = lax.scan(block_step, (ones_row, zero_row, zero_row, zero_row), block_totals)
    carried = prefix(totals, "sp", compose, (ones_row, zero_row, zero_row, zero_row))
    start_re, start_im = (carried[2], carried[3])
    enter_re = before[0] * start_re[None] - before[1] * start_im[None] + before[2]
    enter_im = before[0] * start_im[None] + before[1] * start_re[None] + before[3]
    state_real = local[2] + local[0] * enter_re[None] - local[1] * enter_im[None]
    state_imaginary = local[3] + local[0] * enter_im[None] + local[1] * enter_re[None]
    group_layout_shape = (tok_rows, group_count, state_size)
    state_real = state_real.transpose(1, 0, 2).reshape(group_layout_shape)
    state_imaginary = state_imaginary.transpose(1, 0, 2).reshape(group_layout_shape)
    result = (
        jnp.einsum("hsv,jhv->jhs", output_real, state_real, precision=upper_limit)
        - jnp.einsum("hsv,jhv->jhs", output_imaginary, state_imaginary, precision=upper_limit)
        + skip.reshape(group_count, group_width)[None] * inputs
    )
    return result.reshape(tok_rows, group_count * group_width).astype(jnp.bfloat16)


def attention_branch(queries, keys_local, values_local, mix_weight, head_gain):
    tok_rows = queries.shape[0]
    head_count = mix_weight.shape[0]
    head_dim = queries.shape[1] // (2 * head_count)
    value_dim = values_local.shape[1] // head_count
    scale = head_dim ** (-0.5)
    first_pos = lax.axis_index("sp") * tok_rows
    query_pos = first_pos + jnp.arange(tok_rows, dtype=jnp.int32)
    query_heads = queries.reshape(tok_rows, head_count, 2, head_dim)
    initial = (
        jnp.full((head_count, 2, tok_rows), -1e30, jnp.float32),
        jnp.zeros((head_count, 2, tok_rows), jnp.float32),
        jnp.zeros((head_count, 2, tok_rows, value_dim), jnp.float32),
    )
    key_piece = lax.all_gather(keys_local, "sp", axis=0, tiled=True)
    value_piece = lax.all_gather(values_local, "sp", axis=0, tiled=True)
    count = key_piece.shape[0]
    block = math.gcd(count, 512)

    def one_block(index, inner):
        run_max, run_total, run_accum = inner
        offset = index * block
        key_block = lax.dynamic_slice_in_dim(key_piece, offset, block, 0).reshape(
            block, head_count, 2, head_dim
        )
        value_block = lax.dynamic_slice_in_dim(value_piece, offset, block, 0).reshape(
            block, head_count, value_dim
        )
        key_pos = offset + jnp.arange(block, dtype=jnp.int32)
        scores = (
            jnp.einsum(
                "qhmd,khmd->hmqk", query_heads, key_block, preferred_element_type=jnp.float32
            )
            * scale
        )
        allowed = key_pos[None, :] <= query_pos[:, None]
        masked = jnp.where(allowed, scores, -1e30)
        new_max = jnp.maximum(run_max, jnp.max(masked, axis=-1))
        weights = jnp.where(allowed, jnp.exp(masked - new_max[..., None]), 0.0)
        rescale = jnp.exp(run_max - new_max)
        new_total = run_total * rescale + jnp.sum(weights, axis=-1)
        product = jnp.einsum(
            "hmqk,khd->hmqd",
            weights.astype(jnp.bfloat16),
            value_block,
            preferred_element_type=jnp.float32,
        )
        return (new_max, new_total, run_accum * rescale[..., None] + product)

    def visit(inner):
        return lax.fori_loop(0, count // block, one_block, inner)

    def keep_carry(inner):
        return inner

    maxima, totals, accum = lax.cond(
        jnp.int32(0) <= first_pos + tok_rows - 1, visit, keep_carry, initial
    )
    log_totals = maxima + jnp.log(totals)
    head_raw = (
        accum[:, 0] / totals[:, 0, :, None]
        - mix_weight[:, None, None] * accum[:, 1] / totals[:, 1, :, None]
    )
    normed_heads = (
        head_raw
        * lax.rsqrt(jnp.mean(head_raw * head_raw, axis=-1, keepdims=True) + 1e-05)
        * head_gain
    )
    attn_out = (
        normed_heads.transpose(1, 0, 2)
        .reshape(tok_rows, head_count * value_dim)
        .astype(jnp.bfloat16)
    )
    return (attn_out, log_totals)


def per_device(
    tokens,
    norm_gain,
    w_state_in,
    w_query,
    w_key,
    w_value,
    decay_re,
    decay_im,
    log_step,
    decay_shift,
    in_re,
    in_im,
    output_real,
    output_imaginary,
    skip,
    mix_weight,
    head_gain,
    w_out_state,
    w_out_attn,
):
    whole = lax.all_gather(tokens, "tp", axis=2, tiled=True)[0]
    floats = whole.astype(jnp.float32)
    normed = (
        floats * lax.rsqrt(jnp.mean(floats * floats, axis=-1, keepdims=True) + 1e-06) * norm_gain
    ).astype(jnp.bfloat16)
    pieces = (
        lax.all_gather(w_state_in, ("sp", "fs"), axis=0, tiled=True),
        lax.all_gather(w_query, ("sp", "fs"), axis=0, tiled=True),
        lax.all_gather(w_key, ("sp", "fs"), axis=0, tiled=True),
        lax.all_gather(w_value, ("sp", "fs"), axis=0, tiled=True),
    )
    sums = tuple((jnp.dot(normed, piece, preferred_element_type=jnp.float32) for piece in pieces))
    state_in = sums[0].astype(jnp.bfloat16)
    queries = sums[1].astype(jnp.bfloat16)
    keys_local = sums[2].astype(jnp.bfloat16)
    values_local = sums[3].astype(jnp.bfloat16)
    attn_out, log_totals = attention_branch(
        queries, keys_local, values_local, mix_weight, head_gain
    )
    state_out = state_branch(
        state_in,
        decay_re,
        decay_im,
        log_step,
        decay_shift,
        in_re,
        in_im,
        output_real,
        output_imaginary,
        skip,
    )
    summed = lax.psum_scatter(
        (
            jnp.dot(state_out, w_out_state, preferred_element_type=jnp.float32)
            + jnp.dot(attn_out, w_out_attn, preferred_element_type=jnp.float32)
        ).astype(jnp.bfloat16),
        "tp",
        scatter_dimension=0,
        tiled=True,
    )
    return (summed[None], log_totals[None])


def solution(mesh):
    in_specs = (
        P("fs", "sp", "tp"),
        P(),
        P(("sp", "fs"), "tp"),
        P(("sp", "fs"), "tp"),
        P(("sp", "fs"), "tp"),
        P(("sp", "fs"), "tp"),
        P("tp", None),
        P("tp", None),
        P("tp"),
        P("fs", "tp", "sp"),
        P("tp", None, None),
        P("tp", None, None),
        P("tp", None, None),
        P("tp", None, None),
        P("tp"),
        P("tp"),
        P(),
        P("tp", None),
        P("tp", None),
    )
    out_specs = (P("fs", ("sp", "tp"), None), P("fs", "tp", None, "sp"))
    return jax.shard_map(
        per_device, mesh=mesh, in_specs=in_specs, out_specs=out_specs, check_vma=False
    )
```

profile of v0, /device:TPU:0, one launch (start us, length us, event | category | flops | bytes accessed | tf_op | source)
XLA Modules:
  0.0 575.6 jit_solution(425845792407703568)
XLA Ops:
  14.8 3.5 add.188
  23.2 114.4 %all-gather.14.cloned.1.call-done = bf16[4096,1024]{1,0:T(8,128)(2,1)} async-done(((bf16[256,1024]{1,0:T(8,128)(2,1)}), bf16[4096,1024]{1,0:T(8,128)(2,1)}) %all-gather.14.cloned.1.call-update) | async-done | bytes 8388624 | tf_op jit(solution)/shard_map/all_gather | solution.py:214
  137.6 5.0 convolution_convert_fusion.3
  142.9 3.1 convolution_bitcast_fusion
  147.9 5.7 copy.54
  153.6 4.8 reshape_reshape.9
  158.3 4.5 copy.53
  162.9 4.8 reshape_reshape.8
  167.6 76.2 %while.73 = (s32[]{:T(128)}, f32[8,4096]{1,0:T(8,128)S(1)}, f32[8,4096]{1,0:T(8,128)S(1)}, f32[8,4096]{1,0:T(8,128)S(1)}, f32[8,4096]{1,0:T(8,128)S(1)}, /*index...) while((s32[]{:T(128)}, f32[8,4096]{1,0:T(8,128)S(1)}, ...), condition=%wide.region_2.3_spmd.clone, body=%wide.region_1.0_spmd.clone.sunk | while | flops 589827 | bytes 3146399 | solution.py:84
  243.9 14.0 %while.74 = (s32[]{:T(128)}, f32[4096]{0:T(1024)S(1)}, f32[4096]{0:T(1024)S(1)}, f32[4096]{0:T(1024)S(1)}, f32[4096]{0:T(1024)S(1)}, /*index=5*/f32[8,4096]{1,0:...) while((s32[]{:T(128)}, f32[4096]{0:T(1024)S(1)}, ...), condition=%wide.region_4.5_spmd.clone, body=%wide.region_3.4_spmd.clone.sunk | while | flops 73731 | bytes 655536 | solution.py:93
  257.9 13.9 %all-gather = f32[16384]{0:T(1024)S(1)} all-gather(f32[4096]{0:T(1024)S(1)} %get-tuple-element.345), channel_id=2, replica_groups=mesh['sp'=4,'fs'=4,'tp'=2] {'sp'}, dimensions={0}, use_global_device_ids=true | all-gather | bytes 81920 | tf_op jit(solution)/shard_map/all_gather | solution.py:11
  271.8 13.2 %all-gather.1 = f32[16384]{0:T(1024)S(1)} all-gather(f32[4096]{0:T(1024)S(1)} %get-tuple-element.346), channel_id=3, replica_groups=mesh['sp'=4,'fs'=4,'tp'=2] {'sp'}, dimensions={0}, use_global_device_ids=true | all-gather | bytes 81920 | tf_op jit(solution)/shard_map/all_gather | solution.py:11
  285.0 14.0 %all-gather.2 = f32[16384]{0:T(1024)S(1)} all-gather(f32[4096]{0:T(1024)S(1)} %get-tuple-element.347), channel_id=4, replica_groups=mesh['sp'=4,'fs'=4,'tp'=2] {'sp'}, dimensions={0}, use_global_device_ids=true | all-gather | bytes 81920 | tf_op jit(solution)/shard_map/all_gather | solution.py:11
  299.1 13.6 %all-gather.3 = f32[16384]{0:T(1024)S(1)} all-gather(f32[4096]{0:T(1024)S(1)} %get-tuple-element.348), channel_id=5, replica_groups=mesh['sp'=4,'fs'=4,'tp'=2] {'sp'}, dimensions={0}, use_global_device_ids=true | all-gather | bytes 81920 | tf_op jit(solution)/shard_map/all_gather | solution.py:11
  312.8 6.5 %convolution_convert_fusion.1 = bf16[128,1024]{1,0:T(8,128)(2,1)} fusion(bf16[4096,1024]{1,0:T(8,128)(2,1)} %all-gather.18.cloned.1.call-done, bf16[1,128,4096]{2,1,0:T(8,128)(2,1)S(1)} %copy-done.6, f32[4096]{0:T(1024)S(1)} %copy-done.21, f32[128]{0:T(128)S(1)} %copy-done.24), kind=kOutput, calls=%fused_computation.80 | convolution fusion | flops 1075970048 | bytes 9716224 | tf_op jit(solution)/shard_map/dot_general | solution.py:219
  320.0 4.4 subtract_bitcast_fusion
  326.9 4.6 reshape.86
  331.5 34.0 %all-gather.22.cloned.1.call-done = bf16[4096,1024]{1,0:T(8,128)(2,1)} async-done(((bf16[256,1024]{1,0:T(8,128)(2,1)}), bf16[4096,1024]{1,0:T(8,128)(2,1)}) %all-gather.22.cloned.1.call-update) | async-done | bytes 8388624 | tf_op jit(solution)/shard_map/all_gather | solution.py:217
  365.5 5.7 convolution_convert_fusion
  371.3 11.0 %fusion.20 = f32[64,128,16]{1,2,0:T(8,128)S(1)} fusion(f32[64,16,64]{2,1,0:T(8,128)S(1)} %copy-done, f32[128,64,64]{2,1,0:T(8,128)} %reshape.86), kind=kOutput, calls=%fused_computation.59 | convolution fusion | flops 100663296 | bytes 2883584 | tf_op jit(solution)/shard_map/hsv,jhv->jhs/dot_general | solution.py:105
  384.9 4.7 reshape.85
  389.7 10.9 %fusion.36 = bf16[128,64,16]{0,2,1:T(8,128)(2,1)S(1)} fusion(f32[64,128,16]{1,2,0:T(8,128)S(1)} %fusion.20, f32[64,16,64]{2,1,0:T(8,128)S(1)} %copy-done.7, f32[128,64,64]{2,1,0:T(8,128)} %reshape.85, bf16[128,64,16]{0,2,1:T(8,128)(2,1)S(1)} %bitcast.162, f32[64,16]{1,0:T(8,128)S(1)} %copy-done.10), kind=kOutput, calls=%fused_computation.78 | convolution fusion | flops 101318656 | bytes 3411968 | tf_op jit(solution)/shard_map/hsv,jhv->jhs/dot_general | solution.py:104
  400.6 4.7 fusion.63
  405.3 73.4 %all-gather.16.cloned.1.call-done = bf16[4096,1024]{1,0:T(8,128)(2,1)} async-done(((bf16[256,1024]{1,0:T(8,128)(2,1)}), bf16[4096,1024]{1,0:T(8,128)(2,1)}) %all-gather.16.cloned.1.call-update) | async-done | bytes 8388624 | tf_op jit(solution)/shard_map/all_gather | solution.py:215
  478.7 5.0 convolution_convert_fusion.2
  483.7 23.2 %all-gather.20.cloned.1.call-done = bf16[512,1024]{1,0:T(8,128)(2,1)} async-done(((bf16[128,1024]{1,0:T(8,128)(2,1)}), bf16[512,1024]{1,0:T(8,128)(2,1)}) %all-gather.20.cloned.1.call-update) | async-done | bytes 1048592 | tf_op jit(solution)/shard_map/all_gather | solution.py:125
  506.8 29.0 %all-gather.24.cloned.1.call-done = bf16[512,1024]{1,0:T(8,128)(2,1)} async-done(((bf16[128,1024]{1,0:T(8,128)(2,1)}), bf16[512,1024]{1,0:T(8,128)(2,1)}) %all-gather.24.cloned.1.call-update) | async-done | bytes 1048592 | tf_op jit(solution)/shard_map/all_gather | solution.py:126
  535.8 14.8 %conditional.1 = (f32[4,2,128]{2,1,0:T(2,128)}, f32[4,2,128]{2,1,0:T(2,128)S(1)}, f32[4,2,128,256]{3,2,1,0:T(8,128)}) conditional(s32[]{:T(128)} %convert_element_type.53, () %tuple.43, (s32[]{:T(128)}, s32[128]{0:T(128)S(1)}, bf16[128,1024]{1,0:T(8,128)(2,1)S(1)}, bf16[512,1024]{1,0:T(8,128)(2,1)}, bf16[512,1024]{1,0:T(8,128)(2,1)}) %tuple.44), branch_computations={%region_7.8_spmd, %region_8.11_spmd} | conditional | flops 409800832 | bytes 23115320 | solution.py:166
  535.9 2.8 reshape.78
  546.9 3.7 convolution_add_fusion
  554.7 5.7 fusion.19
  561.7 6.6 %reduce-scatter.2.cloned.1.call-done = bf16[64,4096]{1,0:T(8,128)(2,1)} async-done(((bf16[128,4096]{1,0:T(8,128)(2,1)}), bf16[64,4096]{1,0:T(8,128)(2,1)}) %reduce-scatter.2.cloned.1.call-update) | async-done | bytes 524304 | tf_op jit(solution)/shard_map/reduce_scatter | solution.py:239
  (255 shorter events, 123.1 us)
Async XLA Ops:
  7.2 364.2 %copy-start = (f32[64,16,64]{2,1,0:T(8,128)S(1)}, f32[64,16,64]{2,1,0:T(8,128)}, u32[]{:S(2)}) copy-start(f32[64,16,64]{2,1,0:T(8,128)} %param.40) | copy-start | bytes 786436
  7.2 3.6 copy-start.15
  7.2 3.8 copy-start.22
  7.2 3.9 copy-start.16
  7.2 4.8 copy-start.17
  7.2 14.4 %all-gather.12.cloned.1.call-start = ((), (), s32[]{:S(2)}) async-start(), calls=%async_computation.1 | async-start | bytes 1572864 | tf_op jit(solution)/shard_map/all_gather | solution.py:208
  8.0 129.7 %all-gather.14.cloned.1.call-start = ((), (), s32[]{:S(2)}) async-start(), calls=%async_computation.2 | async-start | bytes 8912896 | tf_op jit(solution)/shard_map/all_gather | solution.py:214
  8.7 304.0 %all-gather.18.cloned.1.call-start = ((), (), s32[]{:S(2)}) async-start(), calls=%async_computation.4 | async-start | bytes 8912896 | tf_op jit(solution)/shard_map/all_gather | solution.py:216
  9.4 356.1 %all-gather.22.cloned.1.call-start = ((), (), s32[]{:S(2)}) async-start(), calls=%async_computation.6 | async-start | bytes 8912896 | tf_op jit(solution)/shard_map/all_gather | solution.py:217
  10.0 468.6 %all-gather.16.cloned.1.call-start = ((), (), s32[]{:S(2)}) async-start(), calls=%async_computation.3 | async-start | bytes 8912896 | tf_op jit(solution)/shard_map/all_gather | solution.py:215
  10.6 496.2 %all-gather.20.cloned.1.call-start = ((), (), s32[]{:S(2)}) async-start(), calls=%async_computation.5 | async-start | bytes 1310720 | tf_op jit(solution)/shard_map/all_gather | solution.py:125
  14.8 3.5 copy-start.18
  19.0 118.6 %copy-start.21 = (f32[4096]{0:T(1024)S(1)}, f32[4096]{0:T(1024)}, u32[]{:S(2)}) copy-start(f32[4096]{0:T(1024)} %param.28) | copy-start | bytes 49156
  23.1 119.5 %copy-start.23 = (f32[128]{0:T(128)}, f32[128]{0:T(128)S(1)}, u32[]{:S(2)}) copy-start(f32[128]{0:T(128)S(1)} %add_rsqrt_fusion.1) | copy-start | bytes 1540
  23.1 119.7 %copy-start.2 = (f32[64,64,16]{1,2,0:T(8,128)S(1)}, f32[64,64,16]{1,2,0:T(8,128)}, u32[]{:S(2)}) copy-start(f32[64,64,16]{1,2,0:T(8,128)} %param.38) | copy-start | bytes 786436
  23.2 119.7 %copy-start.4 = (f32[64,64,16]{1,2,0:T(8,128)S(1)}, f32[64,64,16]{1,2,0:T(8,128)}, u32[]{:S(2)}) copy-start(f32[64,64,16]{1,2,0:T(8,128)} %param.37) | copy-start | bytes 786436
  23.2 119.7 %copy-start.8 = (f32[64,64]{1,0:T(8,128)S(1)}, f32[64,64]{1,0:T(8,128)}, u32[]{:S(2)}) copy-start(f32[64,64]{1,0:T(8,128)} %get-tuple-element.614) | copy-start | bytes 49156
  142.8 3.2 copy-start.3
  142.9 3.2 copy-start.5
  142.9 3.2 copy-start.9
  167.6 76.2 %copy-start.11 = (f32[8,4096]{1,0:T(8,128)S(1)}, f32[8,4096]{1,0:T(8,128)}, u32[]{:S(2)}) copy-start(f32[8,4096]{1,0:T(8,128)} %custom-call.14) | copy-start | bytes 393220
  167.6 76.2 %copy-start.12 = (f32[8,4096]{1,0:T(8,128)S(1)}, f32[8,4096]{1,0:T(8,128)}, u32[]{:S(2)}) copy-start(f32[8,4096]{1,0:T(8,128)} %custom-call.15) | copy-start | bytes 393220
  167.6 76.2 %copy-start.13 = (f32[8,4096]{1,0:T(8,128)S(1)}, f32[8,4096]{1,0:T(8,128)}, u32[]{:S(2)}) copy-start(f32[8,4096]{1,0:T(8,128)} %custom-call.16) | copy-start | bytes 393220
  167.6 76.2 %copy-start.14 = (f32[8,4096]{1,0:T(8,128)S(1)}, f32[8,4096]{1,0:T(8,128)}, u32[]{:S(2)}) copy-start(f32[8,4096]{1,0:T(8,128)} %custom-call.17) | copy-start | bytes 393220
  243.9 68.9 %copy-start.6 = (bf16[1,128,4096]{2,1,0:T(8,128)(2,1)S(1)}, bf16[1,128,4096]{2,1,0:T(8,128)(2,1)}, u32[]{:S(2)}) copy-start(bf16[1,128,4096]{2,1,0:T(8,128)(2,1)} %all-gather.12.cloned.1.call-done) | copy-start | bytes 3145732
  243.9 68.9 %copy-start.24 = (f32[128]{0:T(128)S(1)}, f32[128]{0:T(128)}, u32[]{:S(2)}) copy-start(f32[128]{0:T(128)} %copy-done.23) | copy-start | bytes 1540
  319.9 215.9 %all-gather.24.cloned.1.call-start = ((), (), s32[]{:S(2)}) async-start(), calls=%async_computation.7 | async-start | bytes 1310720 | tf_op jit(solution)/shard_map/all_gather | solution.py:126
  371.3 197.1 %reduce-scatter.2.cloned.1.call-start = ((), (), s32[]{:S(2)}) async-start(), calls=%async_computation.8 | async-start | bytes 1572864 | tf_op jit(solution)/shard_map/reduce_scatter | solution.py:239
  384.9 4.7 copy-start.7
  384.9 4.7 copy-start.10
  550.6 2.6 copy-start.20
  550.6 4.0 copy-start.19
  (1 other events, 1.3 us)
Sparse Core Ops, SparseCore 0:
  9.6 11.7 all-gather.11
  24.1 113.4 all-gather.13
  140.4 110.4 all-gather.17
  253.5 111.9 all-gather.21
  368.2 110.4 all-gather.15
  480.7 26.1 all-gather.19
  508.4 27.3 all-gather.23
  560.6 7.7 reduce-scatter.1
where the time goes:
time: 586 us; the launch traced here: 576 us
  waiting for transfers between devices  284 us (48%)
  local copies, waits for them, and re-layouts  121 us (21%)
  matrix products  65.2 us (11%)
  blocking collectives  54.7 us (9%)
  other arithmetic  33.9 us (6%)
  between operations  15.1 us (3%)
    all_gather x1, waiting for transfers between devices, per_device(): lax.all_gather(w_state_in, ('sp', 'fs'), axis=0, tiled=True)  114 us
    all_gather x1, waiting for transfers between devices, per_device(): lax.all_gather(w_query, ('sp', 'fs'), axis=0, tiled=True)  73.4 us
    dynamic_slice x32, local copies, waits for them, and re-layouts, state_branch(): lax.scan(row_step, (ones_blocks, zero_blocks, zero_blocks, zero_blocks),...  57.1 us
    all_gather x4, blocking collectives, prefix(): everything = jax.tree.map(lambda part: lax.all_gather(part, axis), x)  54.7 us
    all_gather x1, waiting for transfers between devices, per_device(): lax.all_gather(w_value, ('sp', 'fs'), axis=0, tiled=True)  34 us
    all_gather x1, waiting for transfers between devices, attention_branch(): value_piece = lax.all_gather(values_local, 'sp', axis=0, tiled=True)  29 us
    all_gather x1, waiting for transfers between devices, attention_branch(): key_piece = lax.all_gather(keys_local, 'sp', axis=0, tiled=True)  23.2 us
    dot_general x4, matrix products, per_device(): jnp.dot(normed, piece, preferred_element_type=jnp.float32)  22.3 us
  transfers between devices with their start and end apart: 8, of which 6 were waited for; matrix products, arithmetic and copies ran while one was open for 34% of the time, Pallas kernels for 0%

commit v1 on v0

--- a/solution.py
+++ b/solution.py
@@ -1,8 +1,11 @@
+import functools
 import math
 
 import jax
 import jax.numpy as jnp
 from jax import lax
+from jax.experimental import pallas as pl
+from jax.experimental.pallas import tpu as pltpu
 from jax.sharding import PartitionSpec as P
 
 
@@ -248,6 +251,604 @@
     return (summed[None], log_totals[None])
 
 
+def nt_dot(a, b):
+    return lax.dot_general(a, b, (((1,), (1,)), ((), ())), preferred_element_type=jnp.float32)
+
+
+def split_pair(x):
+    high = x.astype(jnp.bfloat16)
+    low = (x - high.astype(jnp.float32)).astype(jnp.bfloat16)
+    return (high, low)
+
+
+def small_expm1(x):
+    total = jnp.ones_like(x)
+    for n in range(9, 1, -1):
+        total = 1.0 + total * x * (1.0 / n)
+    return total * x
+
+
+def fused_kernel(
+    sizes,
+    tok_ref,
+    gain_ref,
+    ws_ref,
+    wq_ref,
+    wk_ref,
+    wv_ref,
+    dre_ref,
+    dim_ref,
+    logstep_ref,
+    shift_ref,
+    inre_ref,
+    inim_ref,
+    outre_ref,
+    outim_ref,
+    skip_ref,
+    mix_ref,
+    hgain_ref,
+    wos_ref,
+    woa_ref,
+    mixed_ref,
+    logt_ref,
+    stat_send,
+    stat_recv,
+    nbuf,
+    xbuf,
+    wbuf,
+    pbuf,
+    rbuf,
+    fin,
+    shsend,
+    shbuf,
+    inbuf,
+    outbuf,
+    coef,
+    etab,
+    bcat,
+    ccat,
+    srow,
+    yacc,
+    stb,
+    atb,
+    sto,
+    ato,
+    ltb,
+    lto,
+    wo,
+    acc,
+    poutb,
+    precb,
+    loc_sem,
+    wo_sem,
+    w_loc,
+    stat_sem,
+    tok_send,
+    tok_recv,
+    fwd_send,
+    wx_send,
+    wx_recv,
+    wy_send,
+    wy_recv,
+    dx_send,
+    dx_recv,
+    dy_send,
+    dy_recv,
+    z_send,
+    z_recv,
+    sh_send,
+    sh_recv,
+    st_send,
+    st_recv,
+    at_send,
+    at_recv,
+    lt_send,
+    lt_recv,
+    p_send,
+    p_recv,
+):
+    NS, NT, L, D, CW = sizes
+    KW = D // NS
+    FW = D // NT
+    NB = NS // NT
+    HC = CW // NS
+    SEQ = NS * L
+    G = HC // 16
+    MESH = pl.DeviceIdType.MESH
+    s, f, c = (lax.axis_index("sp"), lax.axis_index("fs"), lax.axis_index("tp"))
+    fx = f + 1 - 2 * lax.rem(f, 2)
+    fy = lax.rem(f + 2, 4)
+    fd = 3 - f
+    partner = {"tp": 1 - c}
+    owner = s // NB
+
+    def remote(src, dst, send, recv, where):
+        return pltpu.make_async_remote_copy(
+            src_ref=src, dst_ref=dst, send_sem=send, recv_sem=recv, device_id=where, device_id_type=MESH
+        )
+
+    g0 = pl.multiple_of(s * G, G)
+    own_w = [
+        pltpu.make_async_copy(ref, wbuf.at[m, f], w_loc.at[m])
+        for m, ref in enumerate((ws_ref, wq_ref, wk_ref, wv_ref))
+    ]
+    for copy in own_w:
+        copy.start()
+    own_p = [
+        pltpu.make_async_copy(ref.at[pl.ds(g0, G)], dst, loc_sem.at[i])
+        for i, (ref, dst) in enumerate(
+            (
+                (inre_ref, inbuf.at[0]),
+                (inim_ref, inbuf.at[1]),
+                (outre_ref, outbuf.at[0]),
+                (outim_ref, outbuf.at[1]),
+            )
+        )
+    ]
+    for copy in own_p:
+        copy.start()
+    big = [pltpu.make_async_copy(ref, wo.at[i], wo_sem.at[i]) for i, ref in enumerate((wos_ref, woa_ref))]
+    for copy in big:
+        copy.start()
+
+    barrier = pltpu.get_barrier_semaphore()
+    pl.semaphore_signal(barrier, inc=1, device_id={"fs": fx}, device_id_type=MESH)
+    pl.semaphore_signal(barrier, inc=1, device_id={"fs": fy}, device_id_type=MESH)
+    pl.semaphore_signal(barrier, inc=1, device_id=partner, device_id_type=MESH)
+    for k in range(1, NS):
+        pl.semaphore_signal(barrier, inc=1, device_id={"sp": lax.rem(s + k, NS)}, device_id_type=MESH)
+    pl.semaphore_wait(barrier, 2 + NS)
+
+    def own_x(m):
+        return remote(wbuf.at[m, f], wbuf.at[m, f], wx_send.at[m], wx_recv.at[m], {"fs": fx})
+
+    def own_y(m):
+        return remote(wbuf.at[m, f], wbuf.at[m, f], wy_send.at[m], wy_recv.at[m], {"fs": fy})
+
+    half = wbuf.shape[2] // 2
+
+    def fwd_y(m):
+        part = wbuf.at[m, fx, pl.ds(0, half)]
+        return remote(part, part, dy_send.at[m], dy_recv.at[m], {"fs": fy})
+
+    def fwd_x(m):
+        part = wbuf.at[m, fy, pl.ds(half, half)]
+        return remote(part, part, dx_send.at[m], dx_recv.at[m], {"fs": fx})
+
+    tokens = tok_ref[0].astype(jnp.float32)
+    square = jnp.sum(tokens * tokens, axis=1, keepdims=True)
+    stat_send[...] = jnp.broadcast_to(square, (L, 128))
+    stat = remote(stat_send, stat_recv, stat_sem.at[0], stat_sem.at[1], partner)
+    stat.start()
+    for m in range(4):
+        own_w[m].wait()
+    for m in range(2):
+        own_x(m).start()
+        own_y(m).start()
+    for d in range(NS):
+        shsend[d] = shift_ref[0, d * G : (d + 1) * G, :]
+    for k in range(1, NS):
+        d = lax.rem(s + k, NS)
+        remote(shsend.at[d], shbuf.at[s], sh_send.at[d], sh_recv.at[s], {"sp": d}).start()
+    shbuf[s] = shsend[s]
+    stat.wait()
+    mean = (square + stat_recv[:, 0:1]) * (1.0 / D)
+    gain = gain_ref[:, pl.ds(pl.multiple_of(c * FW, FW), FW)]
+    normed = (tok_ref[0].astype(jnp.float32) * lax.rsqrt(mean + 1e-06) * gain).astype(jnp.bfloat16)
+
+    def tok_copy(i):
+        return remote(
+            nbuf.at[i], xbuf.at[s], tok_send.at[i], tok_recv.at[s], {"sp": c * NB + i}
+        )
+
+    for i in range(NB):
+        nbuf[i] = normed[:, i * KW : (i + 1) * KW]
+    for i in range(NB):
+        @pl.when(c * NB + i != s)
+        def _():
+            tok_copy(i).start()
+
+        @pl.when(c * NB + i == s)
+        def _():
+            xbuf[s] = nbuf[i]
+
+    def tok_forward(q):
+        return remote(xbuf.at[q], xbuf.at[q], fwd_send.at[q], tok_recv.at[q], partner)
+
+    def tok_arrival(q):
+        return remote(xbuf.at[q], xbuf.at[q], fwd_send.at[q], tok_recv.at[q], partner)
+
+    re16 = dre_ref[pl.ds(g0, G), :]
+    im16 = dim_ref[pl.ds(g0, G), :]
+    re16 = jnp.concatenate([re16, re16], axis=1)
+    im16 = jnp.concatenate([im16, im16], axis=1)
+    numer_re = small_expm1(re16) * jnp.cos(im16) - 2.0 * jnp.sin(0.5 * im16) ** 2
+    numer_im = jnp.exp(re16) * jnp.sin(im16)
+    modulus = re16 * re16 + im16 * im16
+    coef[0] = re16
+    coef[1] = im16
+    coef[2] = (numer_re * re16 + numer_im * im16) / modulus
+    coef[3] = (numer_im * re16 - numer_re * im16) / modulus
+    for copy in own_p:
+        copy.wait()
+    lane = lax.broadcasted_iota(jnp.int32, (128, 16), 0)
+    chan = lax.broadcasted_iota(jnp.int32, (128, 16), 1)
+    steps = lax.broadcasted_iota(jnp.int32, (L, 128), 0).astype(jnp.float32) + 1.0
+    sel_hi = lax.broadcasted_iota(jnp.int32, (128, 16), 0)
+
+    def table(g, carry):
+        zr = coef[0, pl.ds(g, 1), :]
+        zi = coef[1, pl.ds(g, 1), :]
+        step = jnp.exp(jnp.full((1, 128), logstep_ref[g0 + g], jnp.float32))
+        cr = coef[2, pl.ds(g, 1), :] * step
+        ci = coef[3, pl.ds(g, 1), :] * step
+        angle = steps * zi
+        cosine, sine = (jnp.cos(angle), jnp.sin(angle))
+        shrink = jnp.exp(steps * zr)
+        grow = jnp.exp(-(steps * zr))
+        etab[0, g] = grow * (cosine * cr + sine * ci)
+        etab[1, g] = grow * (cosine * ci - sine * cr)
+        etab[2, g] = shrink * cosine
+        etab[3, g] = shrink * sine
+        pick = (lane == lax.rem(g, 8) * 16 + chan).astype(jnp.bfloat16)
+        ir, ii = (inbuf[0, g], inbuf[1, g])
+        raw = jnp.concatenate([ir, ii, -ii, ir], axis=0)
+        hi, lo = split_pair(raw)
+        bcat[g] = jnp.concatenate(
+            [nt_dot(hi, pick).astype(jnp.bfloat16), nt_dot(lo, pick).astype(jnp.bfloat16)], axis=1
+        )
+        cr_, ci_ = (outbuf[0, g], outbuf[1, g])
+        rawc = jnp.concatenate([cr_, -ci_, -ci_, -cr_], axis=1)
+        hi, lo = split_pair(rawc)
+        ccat[g] = jnp.concatenate(
+            [
+                jnp.dot(pick, hi, preferred_element_type=jnp.float32).astype(jnp.bfloat16),
+                jnp.dot(pick, lo, preferred_element_type=jnp.float32).astype(jnp.bfloat16),
+            ],
+            axis=0,
+        )
+        return carry
+
+    lax.fori_loop(0, G, table, 0)
+    for k in range(1, NS):
+        q = lax.rem(s + k, NS)
+        remote(shsend.at[q], shbuf.at[q], sh_send.at[q], sh_recv.at[q], {"sp": q}).wait_recv()
+    row_i = lax.broadcasted_iota(jnp.int32, (L, L), 0)
+    col_i = lax.broadcasted_iota(jnp.int32, (L, L), 1)
+    upper = (row_i <= col_i).astype(jnp.float32)
+    for k in range(NS):
+        srow[k] = jnp.dot(
+            shbuf[k], upper, precision=lax.Precision.HIGHEST, preferred_element_type=jnp.float32
+        )
+
+    for k in range(NS):
+        q = lax.rem(s + k, NS)
+
+        @pl.when(c == owner)
+        def _():
+            @pl.when(q != s)
+            def _():
+                tok_arrival(q).wait_recv()
+
+            tok_forward(q).start()
+
+        @pl.when(c != owner)
+        def _():
+            tok_arrival(q).wait_recv()
+
+    def z_copy(m, d):
+        return remote(pbuf.at[m, d], rbuf.at[m, s], z_send.at[m, d], z_recv.at[m, s], {"sp": d})
+
+    def project(m, carry):
+        own_x(m).wait_recv()
+        own_y(m).wait_recv()
+        fwd_y(m).start()
+        fwd_x(m).start()
+
+        @pl.when(m < 2)
+        def _():
+            own_x(m + 2).start()
+            own_y(m + 2).start()
+
+        diag_y = wbuf.at[m, fd, pl.ds(0, half)]
+        diag_x = wbuf.at[m, fd, pl.ds(half, half)]
+        remote(diag_y, diag_y, dy_send.at[m], dy_recv.at[m], {"fs": fy}).wait_recv()
+        remote(diag_x, diag_x, dx_send.at[m], dx_recv.at[m], {"fs": fx}).wait_recv()
+
+        def block(k, inner):
+            d = lax.rem(s + k + 1, NS)
+            columns = pl.ds(pl.multiple_of(d * HC, HC), HC)
+            lhs = xbuf[...].reshape(SEQ, KW)
+            rhs = wbuf[m, :, :, columns].reshape(KW, HC)
+            part = jnp.dot(lhs, rhs, preferred_element_type=jnp.float32).astype(jnp.bfloat16)
+
+            @pl.when(k < NS - 1)
+            def _():
+                pbuf[m, d] = part
+                z_copy(m, d).start()
+
+            @pl.when(k == NS - 1)
+            def _():
+                rbuf[m, s] = part
+
+            return inner
+
+        return lax.fori_loop(0, NS, block, carry)
+
+    def finish(m):
+        for k in range(1, NS):
+            q = lax.rem(s + k, NS)
+            remote(pbuf.at[m, q], rbuf.at[m, q], z_send.at[m, q], z_recv.at[m, q], {"sp": q}).wait_recv()
+        total = rbuf[m, 0].astype(jnp.float32)
+        for q in range(1, NS):
+            total = total + rbuf[m, q].astype(jnp.float32)
+        fin[m] = total.astype(jnp.bfloat16)
+
+    lax.fori_loop(0, 2, project, 0)
+
+    finish(0)
+    sign = jnp.where(lax.broadcasted_iota(jnp.int32, (8, 128), 1) < 64, -1.0, 1.0)
+    lower = row_i >= col_i
+
+    def lane_block(b, carry):
+        lanes = pl.ds(pl.multiple_of(b * 128, 128), 128)
+        u = fin[0, :, lanes]
+        uu = jnp.concatenate([u, u], axis=1)
+        yacc[...] = jnp.zeros_like(yacc)
+
+        def group(g8, inner):
+            g = b * 8 + g8
+            drives = nt_dot(uu, bcat[g])
+            h = jnp.zeros((1, 128), jnp.float32)
+            er, ei, fr, fi = (etab[0, g], etab[1, g], etab[2, g], etab[3, g])
+            for k in range(NS):
+                d = drives[k * L : (k + 1) * L]
+                x = er * d[:, :128] + ei * d[:, 128:]
+                xh, xl = split_pair(x)
+                xx = jnp.concatenate([xh, xl], axis=1)
+                rhs = jnp.concatenate([xx, xx], axis=0)
+                sr = jnp.broadcast_to(srow[k, pl.ds(g, 1), :], (L, L))
+                sc = sr.T
+                mask = jnp.where(lower, jnp.exp(jnp.minimum(sc - sr, 0.0)), 0.0)
+                mh, ml = split_pair(mask)
+                w2 = jnp.dot(
+                    jnp.concatenate([mh, ml], axis=1), rhs, preferred_element_type=jnp.float32
+                )
+                q = w2[:, :128] + w2[:, 128:] + jnp.exp(sc) * h
+                p1 = q * fr
+                p2 = q * fi
+                tail = p1[L - 8 :] + sign * pltpu.roll(p2[L - 8 :], 64, 1)
+                h = tail[7:8]
+                ph, plow = split_pair(jnp.concatenate([p1, p2], axis=1))
+                y2 = nt_dot(ph, ccat[g]) + nt_dot(plow, ccat[g])
+                yacc[k * L : (k + 1) * L, :] += y2[:, :128] + y2[:, 128:]
+            return inner
+
+        lax.fori_loop(0, 8, group, 0)
+        direct = skip_ref[:, pl.ds(pl.multiple_of(s * HC + b * 128, 128), 128)]
+        out = (yacc[...] + direct * u.astype(jnp.float32)).astype(jnp.bfloat16)
+        for k in range(NS):
+            stb[k, :, lanes] = out[k * L : (k + 1) * L]
+        return carry
+
+    lax.fori_loop(0, HC // 128, lane_block, 0)
+
+    lax.fori_loop(2, 4, project, 0)
+
+    def st_copy(d):
+        return remote(stb.at[d], sto.at[s], st_send.at[d], st_recv.at[s], {"sp": d})
+
+    def at_copy(d):
+        return remote(atb.at[d], ato.at[s], at_send.at[d], at_recv.at[s], {"sp": d})
+
+    def lt_copy(d):
+        return remote(ltb.at[d], lto.at[s], lt_send.at[d], lt_recv.at[s], {"sp": d})
+
+    for k in range(1, NS):
+        st_copy(lax.rem(s + k, NS)).start()
+    sto[s] = stb[s]
+
+    hd = HC // 2
+    finish(1)
+    finish(2)
+    finish(3)
+    lam = mix_ref[s]
+    for i in range(NS):
+        width = (i + 1) * L
+        heads = []
+        for m in range(2):
+            sc = nt_dot(
+                fin[1, i * L : (i + 1) * L, m * hd : (m + 1) * hd], fin[2, 0:width, m * hd : (m + 1) * hd]
+            ) * (hd ** (-0.5))
+            qpos = lax.broadcasted_iota(jnp.int32, (L, width), 0) + i * L
+            kpos = lax.broadcasted_iota(jnp.int32, (L, width), 1)
+            allowed = kpos <= qpos
+            sc = jnp.where(allowed, sc, -1e30)
+            top = jnp.max(sc, axis=1, keepdims=True)
+            weights = jnp.where(allowed, jnp.exp(sc - top), 0.0)
+            total = jnp.sum(weights, axis=1, keepdims=True)
+            value = jnp.dot(
+                weights.astype(jnp.bfloat16), fin[3, 0:width, :], preferred_element_type=jnp.float32
+            )
+            heads.append(value / total)
+            logs = jnp.broadcast_to(top + jnp.log(total), (L, L)).T
+            ltb[i, m : m + 1, :] = logs[0:1]
+        raw = heads[0] - lam * heads[1]
+        scale = lax.rsqrt(jnp.mean(raw * raw, axis=1, keepdims=True) + 1e-05)
+        atb[i] = (raw * scale * hgain_ref[...]).astype(jnp.bfloat16)
+
+    for k in range(1, NS):
+        d = lax.rem(s + k, NS)
+        at_copy(d).start()
+        lt_copy(d).start()
+    ato[s] = atb[s]
+    lto[s] = ltb[s]
+
+    for copy in big:
+        copy.wait()
+    for k in range(1, NS):
+        q = lax.rem(s + k, NS)
+        remote(stb.at[q], sto.at[q], st_send.at[q], st_recv.at[q], {"sp": q}).wait_recv()
+    tiles = poutb.shape[0]
+    width = D // tiles
+    st_lhs = jnp.concatenate([sto[q] for q in range(NS)], axis=1)
+
+    def state_tile(n, carry):
+        columns = pl.ds(pl.multiple_of(n * width, width), width)
+        acc[:, columns] = jnp.dot(st_lhs, wo[0, :, columns], preferred_element_type=jnp.float32)
+        return carry
+
+    lax.fori_loop(0, tiles, state_tile, 0)
+    for k in range(1, NS):
+        q = lax.rem(s + k, NS)
+        remote(atb.at[q], ato.at[q], at_send.at[q], at_recv.at[q], {"sp": q}).wait_recv()
+    at_lhs = jnp.concatenate([ato[q] for q in range(NS)], axis=1)
+    rows = L // NT
+    mine = pl.ds(pl.multiple_of(c * rows, rows), rows)
+
+    def p_copy(n):
+        theirs = pl.ds(pl.multiple_of((1 - c) * rows, rows), rows)
+        return remote(poutb.at[n, theirs], precb.at[n], p_send.at[n], p_recv.at[n], partner)
+
+    def attn_tile(n, carry):
+        columns = pl.ds(pl.multiple_of(n * width, width), width)
+        part = acc[:, columns] + jnp.dot(at_lhs, wo[1, :, columns], preferred_element_type=jnp.float32)
+        poutb[n] = part.astype(jnp.bfloat16)
+        p_copy(n).start()
+        return carry
+
+    lax.fori_loop(0, tiles, attn_tile, 0)
+
+    def last_tile(n, carry):
+        columns = pl.ds(pl.multiple_of(n * width, width), width)
+        p_copy(n).wait()
+        mixed_ref[0, :, columns] = (
+            poutb[n, mine, :].astype(jnp.float32) + precb[n].astype(jnp.float32)
+        ).astype(jnp.bfloat16)
+        return carry
+
+    lax.fori_loop(0, tiles, last_tile, 0)
+    for k in range(1, NS):
+        q = lax.rem(s + k, NS)
+        remote(ltb.at[q], lto.at[q], lt_send.at[q], lt_recv.at[q], {"sp": q}).wait_recv()
+    logt_ref[0] = lto[...]
+
+    for m in range(4):
+        own_x(m).wait_send()
+        own_y(m).wait_send()
+        fwd_x(m).wait_send()
+        fwd_y(m).wait_send()
+        for k in range(1, NS):
+            z_copy(m, lax.rem(s + k, NS)).wait_send()
+    for k in range(1, NS):
+        d = lax.rem(s + k, NS)
+        remote(shsend.at[d], shbuf.at[s], sh_send.at[d], sh_recv.at[s], {"sp": d}).wait_send()
+        st_copy(d).wait_send()
+        at_copy(d).wait_send()
+        lt_copy(d).wait_send()
+    for i in range(NB):
+        @pl.when(c * NB + i != s)
+        def _():
+            tok_copy(i).wait_send()
+
+    @pl.when(c == owner)
+    def _():
+        for q in range(NS):
+            tok_forward(q).wait_send()
+
+
+def fused_device(sizes, *args):
+    (tokens, norm_gain, ws, wq, wk, wv, dre, dim, logstep, shift, inre, inim, outre, outim, skip, mix, hgain, wos, woa) = args
+    NS, NT, L, D, CW = sizes
+    KW, HC = (D // NS, CW // NS)
+    SEQ, G, NB, NF = (NS * L, HC // 16, NS // NT, 4)
+    tiles = 8
+    bf, f32 = (jnp.bfloat16, jnp.float32)
+    V = pltpu.VMEM
+    DMA = pltpu.SemaphoreType.DMA
+    vmem = pl.BlockSpec(memory_space=pltpu.VMEM)
+    smem = pl.BlockSpec(memory_space=pltpu.SMEM)
+    hbm = pl.BlockSpec(memory_space=pl.ANY)
+    scratch = [
+        V((L, 128), f32),
+        V((L, 128), f32),
+        V((NB, L, KW), bf),
+        V((NS, L, KW), bf),
+        V((4, NF, ws.shape[0], CW), bf),
+        V((4, NS, SEQ, HC), bf),
+        V((4, NS, SEQ, HC), bf),
+        V((4, SEQ, HC), bf),
+        V((NS, G, L), f32),
+        V((NS, G, L), f32),
+        V((2, G, 64, 16), f32),
+        V((2, G, 16, 64), f32),
+        V((4, G, 128), f32),
+        V((4, G, L, 128), f32),
+        V((G, 256, 256), bf),
+        V((G, 256, 256), bf),
+        V((NS, G, L), f32),
+        V((SEQ, 128), f32),
+        V((NS, L, HC), bf),
+        V((NS, L, HC), bf),
+        V((NS, L, HC), bf),
+        V((NS, L, HC), bf),
+        V((NS, 2, L), f32),
+        V((NS, 2, L), f32),
+        V((2, CW, D), bf),
+        V((L, D), f32),
+        V((tiles, L, D // tiles), bf),
+        V((tiles, L // NT, D // tiles), bf),
+        DMA((4,)),
+        DMA((2,)),
+        DMA((4,)),
+        DMA((2,)),
+        DMA((NB,)),
+        DMA((NS,)),
+        DMA((NS,)),
+    ]
+    scratch += [DMA((4,))] * 8
+    scratch += [DMA((4, NS))] * 2
+    scratch += [DMA((NS,))] * 8
+    scratch += [DMA((tiles,))] * 2
+    call = pl.pallas_call(
+        functools.partial(fused_kernel, sizes),
+        out_shape=(
+            jax.ShapeDtypeStruct((1, L // NT, D), bf),
+            jax.ShapeDtypeStruct((1, NS, 2, L), f32),
+        ),
+        in_specs=[vmem, vmem, hbm, hbm, hbm, hbm, vmem, vmem, smem, vmem, hbm, hbm, hbm, hbm, vmem, smem, vmem, hbm, hbm],
+        out_specs=(vmem, vmem),
+        scratch_shapes=scratch,
+        compiler_params=pltpu.CompilerParams(
+            collective_id=0, has_side_effects=True, vmem_limit_bytes=67043328
+        ),
+    )
+    return call(
+        tokens, norm_gain.reshape(1, -1), ws, wq, wk, wv, dre, dim, logstep, shift, inre, inim, outre, outim,
+        skip.reshape(1, -1), mix, hgain.reshape(1, -1), wos, woa,
+    )
+
+
+def choose_device(sp, fs, tp, *args):
+    tokens, ws, dre, inre, mix = (args[0], args[2], args[6], args[10], args[15])
+    L, D = (tokens.shape[1], ws.shape[0] * sp * fs)
+    CW = ws.shape[1]
+    fits = (
+        fs == 4
+        and tp == 2
+        and sp % tp == 0
+        and mix.shape[0] == sp
+        and L == 128
+        and CW == sp * 256
+        and dre.shape == (sp * 16, 64)
+        and inre.shape[2] == 16
+        and D % (sp * 128) == 0
+    )
+    if fits:
+        return fused_device((sp, tp, L, D, CW), *args)
+    return per_device(*args)
+
+
 def solution(mesh):
     in_specs = (
         P("fs", "sp", "tp"),
@@ -271,6 +872,7 @@
         P("tp", None),
     )
     out_specs = (P("fs", ("sp", "tp"), None), P("fs", "tp", None, "sp"))
+    body = functools.partial(choose_device, mesh.shape["sp"], mesh.shape["fs"], mesh.shape["tp"])
     return jax.shard_map(
-        per_device, mesh=mesh, in_specs=in_specs, out_specs=out_specs, check_vma=False
-    )
+        body, mesh=mesh, in_specs=in_specs, out_specs=out_specs, check_vma=False
+    )

time: 586 us -> 163 us (0.28); the launches traced: 576 us -> 162 us
  waiting for transfers between devices: 284 us -> 0 us
  Pallas kernels: 0 us -> 153 us
  local copies, waits for them, and re-layouts: 121 us -> 9.13 us
  matrix products: 65.2 us -> 0 us
  blocking collectives: 54.7 us -> 0 us
  other arithmetic: 33.9 us -> 0 us
  between operations: 15.1 us -> 0.64 us
    all_gather x7 -> x0, waiting for transfers between devices: 274 us -> none  [the longest x1 114 us: per_device(): lax.all_gather(w_state_in, ('sp', 'fs'), axis=0, tiled=True)]
    pallas_call x0 -> x1, Pallas kernels: none -> 153 us  [fused_device(): call(tokens, norm_gain.reshape(1, -1), ws, wq, wk, wv, dre, dim, logstep,...]
    dot_general x12 -> x0, matrix products: 65.2 us -> none  [the longest x4 22.3 us: per_device(): jnp.dot(normed, piece, preferred_element_type=jnp.float32)]
    dynamic_slice x56 -> x0, local copies, waits for them, and re-layouts: 57.9 us -> none  [the longest x32 57.1 us: state_branch(): lax.scan(row_step, (ones_blocks, zero_blocks, zero_blocks, zero_blocks),...]
    all_gather x4 -> x0, blocking collectives: 54.7 us -> none  [prefix(): everything = jax.tree.map(lambda part: lax.all_gather(part, axis), x)]
    dynamic_update_slice x16 -> x0, other arithmetic: 18.6 us -> none  [state_branch(): lax.scan(row_step, (ones_blocks, zero_blocks, zero_blocks, zero_blocks),...]
    transpose x5 -> x0, local copies, waits for them, and re-layouts: 15.4 us -> none  [the longest x1 5.68 us: state_branch(): jnp.einsum('gpc,tgc->tgp', matrix_im, inputs, precision=upper_limit)]
    reshape x5 -> x0, local copies, waits for them, and re-layouts: 15 us -> none  [the longest x1 4.73 us: state_branch(): state_real = state_real.transpose(1, 0, 2).reshape(group_layout_shape)]
  transfers between devices with their start and end apart: 8 -> 0, of which waited for: 6 -> 0; matrix products, arithmetic and copies ran while one was open for 34% -> 0% of each run, Pallas kernels for 0% -> 0%
where the time goes in v1:
time: 163 us; the launch traced here: 162 us
  Pallas kernels  153 us (94%)
  local copies, waits for them, and re-layouts  9.13 us (6%)
    pallas_call x1, Pallas kernels, fused_device(): call(tokens, norm_gain.reshape(1, -1), ws, wq, wk, wv, dre, dim, logstep,...  153 us
    unnamed x4, local copies, waits for them, and re-layouts  9.13 us

profile of v1, /device:TPU:0, one launch (start us, length us, event | category | flops | bytes accessed | tf_op | source)
XLA Modules:
  0.0 162.4 jit_solution(7289717806359256455)
XLA Ops:
  0.6 3.0 %copy.21.inre_ref = f32[64,64,16]{2,1,0:T(8,128)} copy(f32[64,64,16]{1,2,0:T(8,128)} %param.29) | data formatting | bytes 524288 | tf_op args[10]
  3.6 3.0 %copy.22.inim_ref = f32[64,64,16]{2,1,0:T(8,128)} copy(f32[64,64,16]{1,2,0:T(8,128)} %param.30) | data formatting | bytes 524288 | tf_op args[11]
  6.6 152.6 %shard_map.194 = (bf16[1,64,4096]{2,1,0:T(8,128)(2,1)}, f32[1,4,2,128]{3,2,1,0:T(2,128)}) custom-call(bf16[1,128,2048]{2,1,0:T(8,128)(2,1)} %tok_ref.1, f32[1,4096]{1,0:T(1,128)} %bitcast.3, bf16[256,1024]{1,0:T(8,128)(2,1)} %ws_ref.1, bf16[256,1024]{1,0:T(8,128)(2,1)} %wq_ref.1, bf16[256,1024]{1,0:T(8,128)(2,1)} %wk_ref.1, bf16[256,1024]{1,0:T(8,128)(2,1)} %wv_ref.1, ...), custom_call_target="tpu_custom_call" | custom-call | tf_op jit(solution)/shard_map/pallas_call | solution.py:826
  159.2 1.9 %copy.25 = bf16[1,64,4096]{2,1,0:T(8,128)(2,1)} copy(bf16[1,64,4096]{2,1,0:T(8,128)(2,1)} %get-tuple-element.4) | data formatting | bytes 1048576
  161.1 1.3 copy.26

commit v2 on v1

--- a/solution.py
+++ b/solution.py
@@ -309,6 +309,7 @@
     ccat,
     srow,
     yacc,
+    wts,
     stb,
     atb,
     sto,
@@ -335,7 +336,8 @@
     dy_send,
     dy_recv,
     z_send,
-    z_recv,
+    zr_recv,
+    zl_recv,
     sh_send,
     sh_recv,
     st_send,
@@ -492,10 +494,14 @@
         etab[3, g] = shrink * sine
         pick = (lane == lax.rem(g, 8) * 16 + chan).astype(jnp.bfloat16)
         ir, ii = (inbuf[0, g], inbuf[1, g])
-        raw = jnp.concatenate([ir, ii, -ii, ir], axis=0)
+        raw = jnp.concatenate([ir, ii, -ii, ir], axis=1)
         hi, lo = split_pair(raw)
         bcat[g] = jnp.concatenate(
-            [nt_dot(hi, pick).astype(jnp.bfloat16), nt_dot(lo, pick).astype(jnp.bfloat16)], axis=1
+            [
+                jnp.dot(pick, hi, preferred_element_type=jnp.float32).astype(jnp.bfloat16),
+                jnp.dot(pick, lo, preferred_element_type=jnp.float32).astype(jnp.bfloat16),
+            ],
+            axis=0,
         )
         cr_, ci_ = (outbuf[0, g], outbuf[1, g])
         rawc = jnp.concatenate([cr_, -ci_, -ci_, -cr_], axis=1)
@@ -536,8 +542,48 @@
         def _():
             tok_arrival(q).wait_recv()
 
-    def z_copy(m, d):
-        return remote(pbuf.at[m, d], rbuf.at[m, s], z_send.at[m, d], z_recv.at[m, s], {"sp": d})
+    def z_right(m, d):
+        return remote(pbuf.at[m, d], rbuf.at[0, m, d], z_send.at[m, d], zr_recv.at[m, d], {"sp": lax.rem(s + 1, NS)})
+
+    def z_left(m, d):
+        return remote(
+            pbuf.at[m, d], rbuf.at[1, m, d], z_send.at[m, d], zl_recv.at[m, d], {"sp": lax.rem(s + NS - 1, NS)}
+        )
+
+    def hop_right(m, k):
+        d = NS - 1 - k
+
+        @pl.when(d > s)
+        def _():
+            z_right(m, d).wait_recv()
+            pbuf[m, d] = (pbuf[m, d].astype(jnp.float32) + rbuf[0, m, d].astype(jnp.float32)).astype(jnp.bfloat16)
+            z_right(m, d).start()
+
+    def hop_left(m, d):
+        @pl.when(d < s)
+        def _():
+            z_left(m, d).wait_recv()
+            pbuf[m, d] = (pbuf[m, d].astype(jnp.float32) + rbuf[1, m, d].astype(jnp.float32)).astype(jnp.bfloat16)
+            z_left(m, d).start()
+
+    def each(hop, m):
+        def one(k, carry):
+            hop(m, k)
+            return carry
+
+        lax.fori_loop(0, NS, one, 0)
+
+    def relay(m):
+        @pl.when(jnp.logical_and(s > 0, s < NS // 2))
+        def _():
+            each(hop_right, m)
+            each(hop_left, m)
+
+        @pl.when(jnp.logical_and(s >= NS // 2, s < NS - 1))
+        def _():
+            each(hop_left, m)
+            each(hop_right, m)
+
 
     def project(m, carry):
         own_x(m).wait_recv()
@@ -550,41 +596,60 @@
             own_x(m + 2).start()
             own_y(m + 2).start()
 
+        @pl.when(m > 0)
+        def _():
+            relay(m - 1)
+
         diag_y = wbuf.at[m, fd, pl.ds(0, half)]
         diag_x = wbuf.at[m, fd, pl.ds(half, half)]
         remote(diag_y, diag_y, dy_send.at[m], dy_recv.at[m], {"fs": fy}).wait_recv()
         remote(diag_x, diag_x, dx_send.at[m], dx_recv.at[m], {"fs": fx}).wait_recv()
 
         def block(k, inner):
-            d = lax.rem(s + k + 1, NS)
+            d = jnp.where(s < NS // 2, NS - 1 - k, k)
             columns = pl.ds(pl.multiple_of(d * HC, HC), HC)
             lhs = xbuf[...].reshape(SEQ, KW)
             rhs = wbuf[m, :, :, columns].reshape(KW, HC)
             part = jnp.dot(lhs, rhs, preferred_element_type=jnp.float32).astype(jnp.bfloat16)
 
-            @pl.when(k < NS - 1)
+            pbuf[m, d] = part
+
+            @pl.when(jnp.logical_and(s == 0, d > 0))
             def _():
-                pbuf[m, d] = part
-                z_copy(m, d).start()
-
-            @pl.when(k == NS - 1)
+                z_right(m, d).start()
+
+            @pl.when(jnp.logical_and(s == NS - 1, d < NS - 1))
             def _():
-                rbuf[m, s] = part
+                z_left(m, d).start()
 
             return inner
 
         return lax.fori_loop(0, NS, block, carry)
 
     def finish(m):
-        for k in range(1, NS):
-            q = lax.rem(s + k, NS)
-            remote(pbuf.at[m, q], rbuf.at[m, q], z_send.at[m, q], z_recv.at[m, q], {"sp": q}).wait_recv()
-        total = rbuf[m, 0].astype(jnp.float32)
-        for q in range(1, NS):
-            total = total + rbuf[m, q].astype(jnp.float32)
-        fin[m] = total.astype(jnp.bfloat16)
-
-    lax.fori_loop(0, 2, project, 0)
+        @pl.when(s > 0)
+        def _():
+            z_right(m, s).wait_recv()
+
+        @pl.when(s < NS - 1)
+        def _():
+            z_left(m, s).wait_recv()
+
+        own = pbuf[m, s].astype(jnp.float32)
+
+        @pl.when(s == 0)
+        def _():
+            fin[m] = (own + rbuf[1, m, s].astype(jnp.float32)).astype(jnp.bfloat16)
+
+        @pl.when(s == NS - 1)
+        def _():
+            fin[m] = (own + rbuf[0, m, s].astype(jnp.float32)).astype(jnp.bfloat16)
+
+        @pl.when(jnp.logical_and(s > 0, s < NS - 1))
+        def _():
+            fin[m] = (own + rbuf[0, m, s].astype(jnp.float32) + rbuf[1, m, s].astype(jnp.float32)).astype(jnp.bfloat16)
+
+    lax.fori_loop(0, 3, project, 0)
 
     finish(0)
     sign = jnp.where(lax.broadcasted_iota(jnp.int32, (8, 128), 1) < 64, -1.0, 1.0)
@@ -598,7 +663,7 @@
 
         def group(g8, inner):
             g = b * 8 + g8
-            drives = nt_dot(uu, bcat[g])
+            drives = jnp.dot(uu, bcat[g], preferred_element_type=jnp.float32)
             h = jnp.zeros((1, 128), jnp.float32)
             er, ei, fr, fi = (etab[0, g], etab[1, g], etab[2, g], etab[3, g])
             for k in range(NS):
@@ -633,7 +698,7 @@
 
     lax.fori_loop(0, HC // 128, lane_block, 0)
 
-    lax.fori_loop(2, 4, project, 0)
+    lax.fori_loop(3, 4, project, 0)
 
     def st_copy(d):
         return remote(stb.at[d], sto.at[s], st_send.at[d], st_recv.at[s], {"sp": d})
@@ -649,13 +714,13 @@
     sto[s] = stb[s]
 
     hd = HC // 2
+    relay(3)
     finish(1)
     finish(2)
-    finish(3)
     lam = mix_ref[s]
+    totals = []
     for i in range(NS):
         width = (i + 1) * L
-        heads = []
         for m in range(2):
             sc = nt_dot(
                 fin[1, i * L : (i + 1) * L, m * hd : (m + 1) * hd], fin[2, 0:width, m * hd : (m + 1) * hd]
@@ -667,12 +732,23 @@
             top = jnp.max(sc, axis=1, keepdims=True)
             weights = jnp.where(allowed, jnp.exp(sc - top), 0.0)
             total = jnp.sum(weights, axis=1, keepdims=True)
-            value = jnp.dot(
-                weights.astype(jnp.bfloat16), fin[3, 0:width, :], preferred_element_type=jnp.float32
-            )
-            heads.append(value / total)
+            wts[m, i * L : (i + 1) * L, 0:width] = weights.astype(jnp.bfloat16)
+            totals.append(1.0 / total)
             logs = jnp.broadcast_to(top + jnp.log(total), (L, L)).T
             ltb[i, m : m + 1, :] = logs[0:1]
+    for k in range(1, NS):
+        lt_copy(lax.rem(s + k, NS)).start()
+    lto[s] = ltb[s]
+    finish(3)
+    for i in range(NS):
+        width = (i + 1) * L
+        heads = [
+            jnp.dot(
+                wts[m, i * L : (i + 1) * L, 0:width], fin[3, 0:width, :], preferred_element_type=jnp.float32
+            )
+            * totals[2 * i + m]
+            for m in range(2)
+        ]
         raw = heads[0] - lam * heads[1]
         scale = lax.rsqrt(jnp.mean(raw * raw, axis=1, keepdims=True) + 1e-05)
         atb[i] = (raw * scale * hgain_ref[...]).astype(jnp.bfloat16)
@@ -680,9 +756,7 @@
     for k in range(1, NS):
         d = lax.rem(s + k, NS)
         at_copy(d).start()
-        lt_copy(d).start()
     ato[s] = atb[s]
-    lto[s] = ltb[s]
 
     for copy in big:
         copy.wait()
@@ -739,7 +813,7 @@
         fwd_x(m).wait_send()
         fwd_y(m).wait_send()
         for k in range(1, NS):
-            z_copy(m, lax.rem(s + k, NS)).wait_send()
+            z_right(m, lax.rem(s + k, NS)).wait_send()
     for k in range(1, NS):
         d = lax.rem(s + k, NS)
         remote(shsend.at[d], shbuf.at[s], sh_send.at[d], sh_recv.at[s], {"sp": d}).wait_send()
@@ -776,11 +850,11 @@
         V((NS, L, KW), bf),
         V((4, NF, ws.shape[0], CW), bf),
         V((4, NS, SEQ, HC), bf),
-        V((4, NS, SEQ, HC), bf),
+        V((2, 4, NS, SEQ, HC), bf),
         V((4, SEQ, HC), bf),
         V((NS, G, L), f32),
         V((NS, G, L), f32),
-        V((2, G, 64, 16), f32),
+        V((2, G, 16, 64), f32),
         V((2, G, 16, 64), f32),
         V((4, G, 128), f32),
         V((4, G, L, 128), f32),
@@ -788,6 +862,7 @@
         V((G, 256, 256), bf),
         V((NS, G, L), f32),
         V((SEQ, 128), f32),
+        V((2, SEQ, SEQ), bf),
         V((NS, L, HC), bf),
         V((NS, L, HC), bf),
         V((NS, L, HC), bf),
@@ -807,7 +882,7 @@
         DMA((NS,)),
     ]
     scratch += [DMA((4,))] * 8
-    scratch += [DMA((4, NS))] * 2
+    scratch += [DMA((4, NS))] * 3
     scratch += [DMA((NS,))] * 8
     scratch += [DMA((tiles,))] * 2
     call = pl.pallas_call(
@@ -824,7 +899,8 @@
         ),
     )
     return call(
-        tokens, norm_gain.reshape(1, -1), ws, wq, wk, wv, dre, dim, logstep, shift, inre, inim, outre, outim,
+        tokens, norm_gain.reshape(1, -1), ws, wq, wk, wv, dre, dim, logstep, shift,
+        inre.transpose(0, 2, 1), inim.transpose(0, 2, 1), outre, outim,
         skip.reshape(1, -1), mix, hgain.reshape(1, -1), wos, woa,
     )
 

time: 163 us -> 137 us (0.84)
  Pallas kernels: 153 us -> 133 us
  local copies, waits for them, and re-layouts: 9.13 us -> 3.13 us
    pallas_call x1, Pallas kernels: 153 us -> 133 us  [fused_device(): call(tokens, norm_gain.reshape(1, -1), ws, wq, wk, wv, dre, dim, logstep,...]
    unnamed x4 -> x2, local copies, waits for them, and re-layouts: 9.13 us -> 3.13 us
where the time goes in v2:
time: 137 us; the launch traced here: 136 us
  Pallas kernels  133 us (97%)
  local copies, waits for them, and re-layouts  3.13 us (2%)
    pallas_call x1, Pallas kernels, fused_device(): call(tokens, norm_gain.reshape(1, -1), ws, wq, wk, wv, dre, dim, logstep,...  133 us
    unnamed x2, local copies, waits for them, and re-layouts  3.13 us

profile of v2, /device:TPU:0, one launch (start us, length us, event | category | flops | bytes accessed | tf_op | source)
XLA Modules:
  0.0 136.5 jit_solution(17276707903534837685)
XLA Ops:
  0.6 132.7 %shard_map.194 = (bf16[1,64,4096]{2,1,0:T(8,128)(2,1)}, f32[1,4,2,128]{3,2,1,0:T(2,128)}) custom-call(bf16[1,128,2048]{2,1,0:T(8,128)(2,1)} %tok_ref.1, f32[1,4096]{1,0:T(1,128)} %bitcast.7, bf16[256,1024]{1,0:T(8,128)(2,1)} %ws_ref.1, bf16[256,1024]{1,0:T(8,128)(2,1)} %wq_ref.1, bf16[256,1024]{1,0:T(8,128)(2,1)} %wk_ref.1, bf16[256,1024]{1,0:T(8,128)(2,1)} %wv_ref.1, ...), custom_call_target="tpu_custom_call" | custom-call | tf_op jit(solution)/shard_map/pallas_call | solution.py:901
  133.3 1.9 %copy.23 = bf16[1,64,4096]{2,1,0:T(8,128)(2,1)} copy(bf16[1,64,4096]{2,1,0:T(8,128)(2,1)} %get-tuple-element.4) | data formatting | bytes 1048576
  135.2 1.3 copy.24
